TPU v7x, 128 devices: a whole 4x4x4 slice. The times are simulated.
128 devices in a mesh: fs: 16 (over z, x), tp: 8 (over y, core).
Axes of the slice: x: 4, y: 4, z: 4, core: 2. Of those that a mesh axis runs over, the one named last changes fastest.
Arguments:
- tokens: bfloat16 [16384, 2048], P(('fs', 'tp')), may hold values from -6 to 6
- mix_gain: float32 [2048], replicated, may hold values from 0.1 to 1.9
- ffn_gain: float32 [2048], replicated, may hold values from 0.1 to 1.9
- u_weight: float32 [2048, 2048], P('fs', 'tp'), may hold values from -0.125 to 0.125
- u_scale: float32 [2048], P('tp'), may hold values from 0.5 to 2
- v_weight: float32 [2048, 2048], P('fs', 'tp'), may hold values from -0.125 to 0.125
- v_scale: float32 [2048], P('tp'), may hold values from 0.3 to 12
- v_gain: float32 [2048], P('tp'), may hold values from 0.1 to 1.9
- spatial_weight: bfloat16 [8, 128, 128], replicated, may hold values from -0.5 to 0.5
- spatial_bias: float32 [8, 128], replicated, may hold values from 0.1 to 1.9
- out_weight: float32 [2048, 2048], P('tp', 'fs'), may hold values from -0.125 to 0.125
- out_scale: float32 [2048], P('fs'), may hold values from 0.5 to 2
- gate_weight: float32 [2048, 6144], P('fs', 'tp'), may hold values from -0.125 to 0.125
- gate_scale: float32 [6144], P('tp'), may hold values from 0.5 to 2
- up_weight: float32 [2048, 6144], P('fs', 'tp'), may hold values from -0.125 to 0.125
- up_scale: float32 [6144], P('tp'), may hold values from 0.5 to 2
- down_weight: float32 [6144, 2048], P('tp', 'fs'), may hold values from -0.078125 to 0.078125
- down_scale: float32 [2048], P('fs'), may hold values from 0.5 to 2
Outputs:
- layer_out: bfloat16 [16384, 2048], P(('fs', 'tp'))
All inputs are finite; a program needn't handle non-finite values.
Results may differ from a plain program's by a relative error of at most 0.02.
Values may be sent and summed in bfloat16 or wider, within the bound.
A program may use at most 64 MiB of HBM per device.

v0:
```python
import jax
import jax.numpy as jnp
from jax import lax
from jax.sharding import Mesh
from jax.sharding import PartitionSpec as P

A = 2048
A_GROUPS = 8
BLK = 128
TP = ("tp_0", "tp_1")
FS_TP = ("fs", "tp_0", "tp_1")


def copy_for_each(value, axis):
    peers = lax.axis_size(axis)
    return lax.all_to_all(
        jnp.broadcast_to(value[None], (peers, *value.shape)), axis, 0, 0, tiled=True
    )


def laid_out(tiles, dim):
    dims = list(tiles.shape[1:])
    dims[dim] *= tiles.shape[0]
    return jnp.moveaxis(tiles, 0, dim).reshape(dims)


def gather_axes(value, axes, dim):
    far, near = axes
    tiles = copy_for_each(copy_for_each(value, far), near)
    return laid_out(tiles.swapaxes(0, 1).reshape(-1, *value.shape), dim)


def split_up(value, dim, peers):
    dims = value.shape
    tiles = value.reshape(*dims[:dim], peers, dims[dim] // peers, *dims[dim + 1 :])
    return jnp.moveaxis(tiles, dim, 0)


def sent_and_summed(value, axis, dim):
    tiles = split_up(value, dim, lax.axis_size(axis))
    arrived = lax.all_to_all(tiles, axis, split_axis=0, concat_axis=0, tiled=True)
    return arrived.astype(jnp.float32).sum(axis=0)


def sum_in_two_steps(value, axes, dim):
    far, near = axes
    own = sent_and_summed(split_up(value, dim, lax.axis_size(far)), near, dim + 1)
    return jnp.sum(
        lax.all_to_all(own.astype(jnp.bfloat16), far, 0, 0, tiled=True).astype(jnp.float32), axis=0
    )


def turned_gather(arrays, axis, dims):
    turned = [jnp.moveaxis(a, dim, 0) for a, dim in zip(arrays, dims)]
    both = jnp.concatenate([t.reshape(len(t), -1) for t in turned], axis=1)
    out, at, finished = (lax.all_gather(both, axis, axis=0, tiled=True), 0, [])
    for t, dim in zip(turned, dims):
        piece = out[:, at : at + t[0].size].reshape(-1, *t.shape[1:])
        finished.append(jnp.moveaxis(piece, 0, dim))
        at += t[0].size
    return tuple(finished)


def of_everyone(value, axis):
    return copy_for_each(value, axis).sum(axis=0)


def packed_total(arrays, axis):
    ravelled, at, finished = (jnp.concatenate([a.reshape(-1) for a in arrays]), 0, [])
    running = of_everyone(ravelled, axis)
    for a in arrays:
        finished.append(running[at : at + a.size].reshape(a.shape))
        at += a.size
    return tuple(finished)


def rms_rows(values, norm_gain):
    widened = values.astype(jnp.float32)
    factor = lax.rsqrt(jnp.mean(widened * widened, axis=1, keepdims=True) + 1e-06)
    return (widened * factor * norm_gain).astype(jnp.bfloat16)


def collect_rows(shard_rows, project):
    return project(gather_axes(shard_rows, ("tp_0", "tp_1"), 0), jnp.int32(0))


def reduce_rows(term_fn, local_rows):
    return sum_in_two_steps(
        term_fn(jnp.int32(0), local_rows * lax.axis_size(TP)).astype(jnp.bfloat16),
        ("tp_0", "tp_1"),
        0,
    )


def local(
    tokens,
    mix_gain,
    ffn_gain,
    u_weight,
    u_scale,
    v_weight,
    v_scale,
    v_gain,
    spatial_weight,
    spatial_bias,
    out_weight,
    out_scale,
    gate_weight,
    gate_scale,
    up_weight,
    up_scale,
    down_weight,
    down_scale,
):
    local_rows = tokens.shape[0]
    out_columns, down_columns = turned_gather((out_scale, down_scale), "fs", (0, 0))
    u_whole, v_whole, out_whole = turned_gather(
        (
            u_weight.astype(jnp.bfloat16),
            v_weight.astype(jnp.bfloat16),
            out_weight.astype(jnp.bfloat16),
        ),
        "fs",
        (0, 0, 1),
    )
    normed = rms_rows(tokens, mix_gain)

    def project_mixer(segment, offset):
        u_pre = jnp.dot(segment, u_whole, preferred_element_type=jnp.float32) * u_scale
        v_pre = jnp.dot(segment, v_whole, preferred_element_type=jnp.float32) * v_scale
        return jnp.concatenate(
            [jax.nn.gelu(u_pre, approximate=True), jax.nn.gelu(v_pre, approximate=True)], axis=1
        ).astype(jnp.bfloat16)

    joined = collect_rows(normed, project_mixer)
    columns = u_whole.shape[1]
    u_values = joined[:, :columns]
    v_wide = joined[:, columns:].astype(jnp.float32)
    totals, squares = packed_total((jnp.sum(v_wide, axis=1), jnp.sum(v_wide * v_wide, axis=1)), TP)
    average = totals / A
    spread = squares / A - average * average
    v_normed = ((v_wide - average[:, None]) * lax.rsqrt(spread + 1e-05)[:, None] * v_gain).astype(
        jnp.bfloat16
    )
    group_dim = A // A_GROUPS
    groups = columns // group_dim
    first_group = lax.axis_index(TP) * groups
    weights = lax.dynamic_slice_in_dim(spatial_weight, first_group, groups, 0)
    offsets = lax.dynamic_slice_in_dim(spatial_bias, first_group, groups, 0)
    causal = jnp.tril(jnp.ones((BLK, BLK), dtype=bool))
    masked = jnp.where(causal[None], weights, jnp.zeros_like(weights))
    blocks = v_normed.reshape(-1, BLK, groups, group_dim)
    mixed_sum = jnp.einsum("gts,bsgd->btgd", masked, blocks, preferred_element_type=jnp.float32)
    mixed_sum = mixed_sum + offsets.T[None, :, :, None]
    gated_rows = (u_values.reshape(blocks.shape).astype(jnp.float32) * mixed_sum).astype(
        jnp.bfloat16
    )
    gated_rows = gated_rows.reshape(-1, columns)

    def mixer_term(offset, amount):
        return jnp.dot(gated_rows, out_whole, preferred_element_type=jnp.float32) * out_columns

    residual = (tokens.astype(jnp.float32) + reduce_rows(mixer_term, local_rows)).astype(
        jnp.bfloat16
    )
    gate_whole, up_whole, down_whole = turned_gather(
        (
            gate_weight.astype(jnp.bfloat16),
            up_weight.astype(jnp.bfloat16),
            down_weight.astype(jnp.bfloat16),
        ),
        "fs",
        (0, 0, 1),
    )
    normed_second = rms_rows(residual, ffn_gain)

    def project_ffn(segment, offset):
        gate_pre = jnp.dot(segment, gate_whole, preferred_element_type=jnp.float32) * gate_scale
        up_pre = jnp.dot(segment, up_whole, preferred_element_type=jnp.float32) * up_scale
        return (jax.nn.silu(gate_pre) * up_pre).astype(jnp.bfloat16)

    hidden = collect_rows(normed_second, project_ffn)

    def ffn_term(offset, amount):
        return jnp.dot(hidden, down_whole, preferred_element_type=jnp.float32) * down_columns

    return (residual.astype(jnp.float32) + reduce_rows(ffn_term, local_rows)).astype(jnp.bfloat16)


def solution(mesh):
    torus = Mesh(mesh.devices.reshape(mesh.shape["fs"], 4, 2), ("fs", "tp_0", "tp_1"))
    in_specs = (
        P(FS_TP, None),
        P(),
        P(),
        P("fs", TP),
        P(TP),
        P("fs", TP),
        P(TP),
        P(TP),
        P(),
        P(),
        P(TP, "fs"),
        P("fs"),
        P("fs", TP),
        P(TP),
        P("fs", TP),
        P(TP),
        P(TP, "fs"),
        P("fs"),
    )
    out_specs = P(FS_TP, None)
    return jax.shard_map(local, mesh=torus, in_specs=in_specs, out_specs=out_specs, check_vma=False)
```

profile of v0, /device:TPU:1, one launch (start us, length us, event | category | flops | bytes accessed | tf_op | source)
XLA Modules:
  0.0 238.5 jit_solution(4988067022852905276)
XLA Ops:
  11.5 1.2 copy.50
  15.0 1.6 broadcast_in_dim.13
  16.6 5.0 %all-to-all-start = ((bf16[4,128,2048]{2,1,0:T(8,128)(2,1)}), bf16[4,128,2048]{2,1,0:T(8,128)(2,1)S(1)}, u32[]{:S(2)}, u32[]{:S(2)}) async-start(bf16[4,128,2048]{2,1,0:T(8,128)(2,1)} %broadcast_in_dim.13), calls=%async_computation | async-start | bytes 4194304 | tf_op jit(solution)/shard_map/all_to_all | solution.py:16
  21.6 21.1 %all_gather.10 = f32[2048,2]{0,1:T(2,128)S(1)} all-gather(f32[128,2]{0,1:T(2,128)S(1)} %pad_maximum_fusion.3), channel_id=1, replica_groups=mesh['fs'=16,'tp_0'=4,'tp_1'=2] {'fs'}, dimensions={0}, use_global_device_ids=true | all-gather | bytes 17408 | tf_op jit(solution)/shard_map/all_gather | solution.py:56
  42.7 4.3 %all-to-all-done = bf16[4,128,2048]{2,1,0:T(8,128)(2,1)S(1)} async-done(((bf16[4,128,2048]{2,1,0:T(8,128)(2,1)}), bf16[4,128,2048]{2,1,0:T(8,128)(2,1)S(1)}, u32[]{:S(2)}, u32[]{:S(2)}) %all-to-all-start) | async-done | bytes 2097184 | tf_op jit(solution)/shard_map/all_to_all | solution.py:16
  47.6 8.5 %all_to_all.46 = bf16[2,4,128,2048]{3,2,1,0:T(8,128)(2,1)S(1)} all-to-all(bf16[2,4,128,2048]{3,2,1,0:T(8,128)(2,1)S(1)} %broadcast_in_dim.14), channel_id=1, replica_groups=mesh['fs'=16,'tp_0'=4,'tp_1'=2] {'tp_1'}, dimensions={0} | all-to-all | bytes 8388608 | tf_op jit(solution)/shard_map/all_to_all | solution.py:16
  56.1 2.4 copy.43
  58.5 5.7 %all-gather.3.cloned.1.call-done = bf16[2048,768]{0,1:T(8,128)(2,1)} async-done(((bf16[128,768]{0,1:T(8,128)(2,1)}), bf16[2048,768]{0,1:T(8,128)(2,1)}) %all-gather.3.cloned.1.call-update) | async-done | bytes 3145744 | tf_op jit(solution)/shard_map/all_gather | solution.py:56
  64.2 4.1 %convert_reduce_fusion.2 = (f32[1024]{0:T(1024)S(1)}, f32[1024]{0:T(1024)S(1)}, bf16[1024,256]{1,0:T(8,128)(2,1)S(1)}) fusion(f32[256]{0:T(256)S(1)} %copy-done.10, bf16[1024,2048]{1,0:T(8,128)(2,1)} %bitcast.56, bf16[2048,768]{0,1:T(8,128)(2,1)} %all-gather.3.cloned.1.call-done), kind=kOutput, calls=%fused_computation.17 | convolution fusion | flops 1077409792 | bytes 5776384 | tf_op jit(solution)/shard_map/dot_general | solution.py:130
  69.1 6.3 %all-to-all-start.2 = ((f32[8,1,2048]{2,1,0:T(1,128)}), f32[8,1,2048]{2,1,0:T(1,128)S(1)}, u32[]{:S(2)}, u32[]{:S(2)}) async-start(f32[8,1,2048]{2,1,0:T(1,128)} %broadcast_in_dim.15), calls=%async_computation.2 | async-start | bytes 131072 | tf_op jit(solution)/shard_map/all_to_all | solution.py:16
  75.4 4.4 %fusion.24 = bf16[1024,256]{1,0:T(8,128)(2,1)S(1)} fusion(bf16[1024,2048]{1,0:T(8,128)(2,1)} %bitcast.57, bf16[2048,768]{0,1:T(8,128)(2,1)} %all-gather.3.cloned.1.call-done, f32[256]{0:T(256)S(1)} %copy-done.11), kind=kOutput, calls=%fused_computation.41 | convolution fusion | flops 1076363264 | bytes 5768192 | tf_op jit(solution)/shard_map/dot_general | solution.py:129
  81.7 2.5 %multiply_convert_fusion.1 = bf16[1024,2048]{1,0:T(8,128)(2,1)S(1)} fusion(bf16[1024,256]{1,0:T(8,128)(2,1)S(1)} %bitcast.64, f32[2048]{0:T(1024)S(1)} %bitcast.66, bf16[2048,768]{0,1:T(8,128)(2,1)} %all-gather.3.cloned.1.call-done), kind=kOutput, calls=%fused_computation.1 | convolution fusion | flops 1077936128 | bytes 5775360 | tf_op jit(solution)/shard_map/dot_general | solution.py:161
  84.8 8.5 %all_to_all.47 = bf16[2,4,128,2048]{3,2,1,0:T(8,128)(2,1)} all-to-all(bf16[2,4,128,2048]{3,2,1,0:T(8,128)(2,1)S(1)} %bitcast.54), channel_id=1, replica_groups=mesh['fs'=16,'tp_0'=4,'tp_1'=2] {'tp_1'}, dimensions={0} | all-to-all | bytes 8388608 | tf_op jit(solution)/shard_map/all_to_all | solution.py:41
  93.3 3.5 %reduce_sum.91 = bf16[4,128,2048]{2,1,0:T(8,128)(2,1)S(1)} reduce(bf16[2,4,128,2048]{3,2,1,0:T(8,128)(2,1)} %all_to_all.47, bf16[]{:T(256)} %constant.43.clone.1), dimensions={0}, to_apply=%region_4.5 | reduce | flops 1048576 | bytes 6291458 | tf_op jit(solution)/shard_map/reduce_sum | solution.py:42
  96.9 28.6 %all_to_all.48 = bf16[4,128,2048]{2,1,0:T(8,128)(2,1)S(1)} all-to-all(bf16[4,128,2048]{2,1,0:T(8,128)(2,1)S(1)} %reduce_sum.91), channel_id=1, replica_groups=mesh['fs'=16,'tp_0'=4,'tp_1'=2] {'tp_0'}, dimensions={0} | all-to-all | bytes 4194304 | tf_op jit(solution)/shard_map/all_to_all | solution.py:49
  126.6 27.1 %all_to_all.49 = bf16[4,128,2048]{2,1,0:T(8,128)(2,1)S(1)} all-to-all(bf16[4,128,2048]{2,1,0:T(8,128)(2,1)S(1)} %broadcast_in_dim.17), channel_id=1, replica_groups=mesh['fs'=16,'tp_0'=4,'tp_1'=2] {'tp_0'}, dimensions={0} | all-to-all | bytes 4194304 | tf_op jit(solution)/shard_map/all_to_all | solution.py:16
  154.2 9.4 %all_to_all.50 = bf16[2,4,128,2048]{3,2,1,0:T(8,128)(2,1)S(1)} all-to-all(bf16[2,4,128,2048]{3,2,1,0:T(8,128)(2,1)S(1)} %broadcast_in_dim.18), channel_id=1, replica_groups=mesh['fs'=16,'tp_0'=4,'tp_1'=2] {'tp_1'}, dimensions={0} | all-to-all | bytes 8388608 | tf_op jit(solution)/shard_map/all_to_all | solution.py:16
  163.7 2.4 copy.48
  166.1 8.2 %fusion.1 = f32[1024,768]{1,0:T(8,128)} fusion(bf16[1024,2048]{1,0:T(8,128)(2,1)} %bitcast.58, bf16[2048,2304]{0,1:T(8,128)(2,1)} %all-gather.5.cloned.1.call-done), kind=kOutput, calls=%fused_computation.7 | convolution fusion | flops 3221225472 | bytes 10485760 | tf_op jit(solution)/shard_map/dot_general | solution.py:179
  174.3 13.4 %multiply_convert_fusion = bf16[1024,2048]{1,0:T(8,128)(2,1)} fusion(f32[2048]{0:T(1024)S(1)} %bitcast.65, bf16[2048,2304]{0,1:T(8,128)(2,1)} %all-gather.5.cloned.1.call-done, f32[1024,768]{1,0:T(8,128)} %fusion.1, bf16[1024,2048]{1,0:T(8,128)(2,1)} %bitcast.59, f32[768]{0:T(1024)S(1)} %copy-done.8, f32[768]{0:T(1024)S(1)} %copy-done.9), kind=kOutput, calls=%fused_computation | convolution fusion | flops 6452936704 | bytes 17840128 | tf_op jit(solution)/shard_map/dot_general | solution.py:185
  187.7 2.5 %copy.57 = bf16[4,2,128,2048]{3,2,0,1:T(8,128)(2,1)S(1)} copy(bf16[4,2,128,2048]{3,2,1,0:T(8,128)(2,1)} %bitcast.60) | data formatting | bytes 8388608 | tf_op jit(solution)/shard_map/reshape;reshape | solution.py:35
  190.2 8.1 %all_to_all.51 = bf16[2,4,128,2048]{3,2,1,0:T(8,128)(2,1)} all-to-all(bf16[2,4,128,2048]{3,2,1,0:T(8,128)(2,1)S(1)} %bitcast.55), channel_id=1, replica_groups=mesh['fs'=16,'tp_0'=4,'tp_1'=2] {'tp_1'}, dimensions={0} | all-to-all | bytes 8388608 | tf_op jit(solution)/shard_map/all_to_all | solution.py:41
  198.3 3.5 %reduce_sum.94 = bf16[4,128,2048]{2,1,0:T(8,128)(2,1)S(1)} reduce(bf16[2,4,128,2048]{3,2,1,0:T(8,128)(2,1)} %all_to_all.51, bf16[]{:T(256)} %constant.43.clone.1), dimensions={0}, to_apply=%region_7.8 | reduce | flops 1048576 | bytes 6291458 | tf_op jit(solution)/shard_map/reduce_sum | solution.py:42
  201.9 28.5 %all_to_all.52 = bf16[4,128,2048]{2,1,0:T(8,128)(2,1)S(1)} all-to-all(bf16[4,128,2048]{2,1,0:T(8,128)(2,1)S(1)} %reduce_sum.94), channel_id=1, replica_groups=mesh['fs'=16,'tp_0'=4,'tp_1'=2] {'tp_0'}, dimensions={0} | all-to-all | bytes 4194304 | tf_op jit(solution)/shard_map/all_to_all | solution.py:49
  (59 shorter events, 13.9 us)
Async XLA Ops:
  6.5 36.1 %copy-start = (f32[8,128]{1,0:T(8,128)S(1)}, f32[8,128]{1,0:T(8,128)}, u32[]{:S(2)}) copy-start(f32[8,128]{1,0:T(8,128)} %param.27) | copy-start | bytes 12292
  6.5 8.0 %copy-start.2 = (bf16[128,2048]{1,0:T(8,128)(2,1)S(1)}, bf16[128,2048]{1,0:T(8,128)(2,1)}, u32[]{:S(2)}) copy-start(bf16[128,2048]{1,0:T(8,128)(2,1)} %param.18) | copy-start | bytes 1572868
  6.5 8.2 %copy-start.3 = (f32[2048]{0:T(1024)S(1)}, f32[2048]{0:T(1024)}, u32[]{:S(2)}) copy-start(f32[2048]{0:T(1024)} %param.19) | copy-start | bytes 24580
  6.5 57.7 %all-gather.3.cloned.1.call-start = ((), (), s32[]{:S(2)}) async-start(), calls=%async_computation.9 | async-start | bytes 3342336 | tf_op jit(solution)/shard_map/all_gather | solution.py:56
  10.3 155.8 %all-gather.5.cloned.1.call-start = ((), (), s32[]{:S(2)}) async-start(), calls=%async_computation.10 | async-start | bytes 10027008 | tf_op jit(solution)/shard_map/all_gather | solution.py:56
  15.0 6.6 %copy-start.6 = (f32[128]{0:T(128)S(1)}, f32[128]{0:T(128)}, u32[]{:S(2)}) copy-start(f32[128]{0:T(128)} %param.35) | copy-start | bytes 1540
  15.0 6.6 %copy-start.7 = (f32[128]{0:T(128)S(1)}, f32[128]{0:T(128)}, u32[]{:S(2)}) copy-start(f32[128]{0:T(128)} %param.29) | copy-start | bytes 1540
  16.6 30.5 %all-to-all-start = ((bf16[4,128,2048]{2,1,0:T(8,128)(2,1)}), bf16[4,128,2048]{2,1,0:T(8,128)(2,1)S(1)}, u32[]{:S(2)}, u32[]{:S(2)}) async-start(bf16[4,128,2048]{2,1,0:T(8,128)(2,1)} %broadcast_in_dim.13), calls=%async_computation | async-start | bytes 4194304 | tf_op jit(solution)/shard_map/all_to_all | solution.py:16
  56.1 8.1 %copy-start.10 = (f32[256]{0:T(256)S(1)}, f32[256]{0:T(256)}, u32[]{:S(2)}) copy-start(f32[256]{0:T(256)} %param.24) | copy-start | bytes 3076
  64.2 11.2 %copy-start.11 = (f32[256]{0:T(256)S(1)}, f32[256]{0:T(256)}, u32[]{:S(2)}) copy-start(f32[256]{0:T(256)} %param.22) | copy-start | bytes 3076
  69.1 11.2 %all-to-all-start.2 = ((f32[8,1,2048]{2,1,0:T(1,128)}), f32[8,1,2048]{2,1,0:T(1,128)S(1)}, u32[]{:S(2)}, u32[]{:S(2)}) async-start(f32[8,1,2048]{2,1,0:T(1,128)} %broadcast_in_dim.15), calls=%async_computation.2 | async-start | bytes 131072 | tf_op jit(solution)/shard_map/all_to_all | solution.py:16
  75.4 4.9 %copy-start.5 = (f32[256]{0:T(256)S(1)}, f32[256]{0:T(256)}, u32[]{:S(2)}) copy-start(f32[256]{0:T(256)} %param.25) | copy-start | bytes 3076
  125.5 0.7 copy-start.4
  166.1 8.2 %copy-start.8 = (f32[768]{0:T(1024)S(1)}, f32[768]{0:T(1024)}, u32[]{:S(2)}) copy-start(f32[768]{0:T(1024)} %param.33) | copy-start | bytes 9220
  166.1 8.2 %copy-start.9 = (f32[768]{0:T(1024)S(1)}, f32[768]{0:T(1024)}, u32[]{:S(2)}) copy-start(f32[768]{0:T(1024)} %param.31) | copy-start | bytes 9220
  201.8 29.9 %copy-start.1 = (f32[8,128]{1,0:T(8,128)S(1)}, f32[8,128]{1,0:T(8,128)}, u32[]{:S(2)}) copy-start(f32[8,128]{1,0:T(8,128)} %param.27) | copy-start | bytes 12292
Sparse Core Ops, SparseCore 0:
  10.4 53.7 all-gather.2
  66.3 81.8 all-gather.4
where the time goes:
time: 240 us; the launch traced here: 239 us
  blocking collectives  140 us (58%)
  matrix products  33.7 us (14%)
  local copies, waits for them, and re-layouts  15.9 us (7%)
  between operations  13.6 us (6%)
  other arithmetic  13.5 us (6%)
  starting transfers between devices  11.4 us (5%)
  waiting for transfers between devices  10.6 us (4%)
    all_to_all x2, blocking collectives, sum_in_two_steps(): lax.all_to_all(own.astype(jnp.bfloat16), far, 0, 0, tiled=True)  57.1 us
    all_to_all x3, blocking collectives, copy_for_each(): lax.all_to_all(jnp.broadcast_to(value[None], (peers, *value.shape)), axis...  45.1 us
    all_gather x1, blocking collectives, turned_gather(): out, at, finished = (lax.all_gather(both, axis, axis=0, tiled=True), 0, [])  21.1 us
    all_to_all x2, blocking collectives, sent_and_summed(): lax.all_to_all(tiles, axis, split_axis=0, concat_axis=0, tiled=True)  16.7 us
    dot_general x1, matrix products, ffn_term(): jnp.dot(hidden, down_whole, preferred_element_type=jnp.float32)  13.4 us
    all_to_all x2, starting transfers between devices, copy_for_each(): lax.all_to_all(jnp.broadcast_to(value[None], (peers, *value.shape)), axis...  11.3 us
    dot_general x1, matrix products, project_ffn(): jnp.dot(segment, up_whole, preferred_element_type=jnp.float32) * up_scale  8.24 us
    reduce_sum x2, other arithmetic, sent_and_summed(): return arrived.astype(jnp.float32).sum(axis=0)  7.1 us
  transfers between devices with their start and end apart: 4, of which 3 were waited for; matrix products, arithmetic and copies ran while one was open for 13% of the time, Pallas kernels for 0%

commit v1 on v0

--- a/solution.py
+++ b/solution.py
@@ -53,7 +53,13 @@
 def turned_gather(arrays, axis, dims):
     turned = [jnp.moveaxis(a, dim, 0) for a, dim in zip(arrays, dims)]
     both = jnp.concatenate([t.reshape(len(t), -1) for t in turned], axis=1)
-    out, at, finished = (lax.all_gather(both, axis, axis=0, tiled=True), 0, [])
+    out, at, finished = (
+        jnp.concatenate(
+            lax.all_to_all(jnp.stack([both] * lax.axis_size(axis)), axis, 0, 0), axis=0
+        ),
+        0,
+        [],
+    )
     for t, dim in zip(turned, dims):
         piece = out[:, at : at + t[0].size].reshape(-1, *t.shape[1:])
         finished.append(jnp.moveaxis(piece, 0, dim))

time: 240 us -> 432 us (1.80)
  waiting for transfers between devices: 10.6 us -> 228 us
  blocking collectives: 140 us -> 96.3 us
  starting transfers between devices: 11.4 us -> 29.4 us
  between operations: 13.6 us -> 0.32 us
  local copies, waits for them, and re-layouts: 15.9 us -> 27.8 us
    all_to_all x0 -> x3, waiting for transfers between devices: none -> 184 us  [turned_gather(): lax.all_to_all(jnp.stack([both] * lax.axis_size(axis)), axis, 0, 0)]
    all_to_all x2 -> x3, waiting for transfers between devices: 4.82 us -> 44.1 us  [copy_for_each(): lax.all_to_all(jnp.broadcast_to(value[None], (peers, *value.shape)), axis...]
    all_to_all x3 -> x2, blocking collectives: 45.1 us -> 21.5 us  [copy_for_each(): lax.all_to_all(jnp.broadcast_to(value[None], (peers, *value.shape)), axis...]
    all_gather x1 -> x0, blocking collectives: 21.1 us -> none  [turned_gather(): out, at, finished = (lax.all_gather(both, axis, axis=0, tiled=True), 0, [])]
    all_to_all x0 -> x3, starting transfers between devices: none -> 17.1 us  [turned_gather(): lax.all_to_all(jnp.stack([both] * lax.axis_size(axis)), axis, 0, 0)]
    another operation x0 -> x3, local copies, waits for them, and re-layouts: none -> 7.22 us  [turned_gather(): jnp.stack([both] * lax.axis_size(axis))]
    all_gather x2 -> x0, waiting for transfers between devices: 5.74 us -> none  [turned_gather(): out, at, finished = (lax.all_gather(both, axis, axis=0, tiled=True), 0, [])]
    all_to_all x2, local copies, waits for them, and re-layouts: 4.76 us -> 9.5 us  [copy_for_each(): lax.all_to_all(jnp.broadcast_to(value[None], (peers, *value.shape)), axis...]
  transfers between devices with their start and end apart: 4 -> 6, of which waited for: 3 -> 6; matrix products, arithmetic and copies ran while one was open for 13% -> 5% of each run, Pallas kernels for 0% -> 0%
where the time goes in v1:
time: 432 us; the launch traced here: 431 us
  waiting for transfers between devices  228 us (53%)
  blocking collectives  96.3 us (22%)
  matrix products  33.1 us (8%)
  starting transfers between devices  29.4 us (7%)
  local copies, waits for them, and re-layouts  27.8 us (6%)
  other arithmetic  15.7 us (4%)
    all_to_all x3, waiting for transfers between devices, turned_gather(): lax.all_to_all(jnp.stack([both] * lax.axis_size(axis)), axis, 0, 0)  184 us
    all_to_all x2, blocking collectives, sum_in_two_steps(): lax.all_to_all(own.astype(jnp.bfloat16), far, 0, 0, tiled=True)  57.3 us
    all_to_all x3, waiting for transfers between devices, copy_for_each(): lax.all_to_all(jnp.broadcast_to(value[None], (peers, *value.shape)), axis...  44.1 us
    all_to_all x2, blocking collectives, copy_for_each(): lax.all_to_all(jnp.broadcast_to(value[None], (peers, *value.shape)), axis...  21.5 us
    all_to_all x2, blocking collectives, sent_and_summed(): lax.all_to_all(tiles, axis, split_axis=0, concat_axis=0, tiled=True)  17.6 us
    all_to_all x3, starting transfers between devices, turned_gather(): lax.all_to_all(jnp.stack([both] * lax.axis_size(axis)), axis, 0, 0)  17.1 us
    dot_general x1, matrix products, ffn_term(): jnp.dot(hidden, down_whole, preferred_element_type=jnp.float32)  13.3 us
    all_to_all x3, starting transfers between devices, copy_for_each(): lax.all_to_all(jnp.broadcast_to(value[None], (peers, *value.shape)), axis...  12.3 us
  transfers between devices with their start and end apart: 6, of which 6 were waited for; matrix products, arithmetic and copies ran while one was open for 5% of the time, Pallas kernels for 0%

profile of v1, /device:TPU:1, one launch (start us, length us, event | category | flops | bytes accessed | tf_op | source)
XLA Modules:
  0.0 430.6 jit_solution(3424249766580630812)
XLA Ops:
  1.3 8.4 %all-to-all-start.4 = ((f32[16,128,2]{1,2,0:T(2,128)}), f32[16,128,2]{1,2,0:T(2,128)S(1)}, u32[]{:S(2)}, u32[]{:S(2)}) async-start(f32[16,128,2]{1,2,0:T(2,128)} %stack.7), calls=%async_computation.4 | async-start | bytes 32768 | tf_op jit(solution)/shard_map/all_to_all | solution.py:58
  12.2 3.9 all-to-all-done.4
  17.8 4.2 all-to-all-start
  22.4 23.6 %all-to-all-done = bf16[4,128,2048]{2,1,0:T(8,128)(2,1)S(1)} async-done(((bf16[4,128,2048]{2,1,0:T(8,128)(2,1)}), bf16[4,128,2048]{2,1,0:T(8,128)(2,1)S(1)}, u32[]{:S(2)}, u32[]{:S(2)}) %all-to-all-start) | async-done | bytes 2097184 | tf_op jit(solution)/shard_map/all_to_all | solution.py:16
  46.5 11.0 %all_to_all.61 = bf16[2,4,128,2048]{3,2,1,0:T(8,128)(2,1)} all-to-all(bf16[2,4,128,2048]{3,2,1,0:T(8,128)(2,1)S(1)} %broadcast_in_dim.14), channel_id=1, replica_groups=mesh['fs'=16,'tp_0'=4,'tp_1'=2] {'tp_1'}, dimensions={0} | all-to-all | bytes 8388608 | tf_op jit(solution)/shard_map/all_to_all | solution.py:16
  59.6 3.7 all-to-all-start.2
  63.4 4.7 %copy.52 = bf16[2,4,128,2048]{3,2,0,1:T(8,128)(2,1)} copy(bf16[2,4,128,2048]{3,2,1,0:T(8,128)(2,1)} %all_to_all.61) | data formatting | bytes 8388608 | tf_op jit(solution)/shard_map/all_to_all | solution.py:16
  68.1 43.3 %all-to-all-done.2 = bf16[16,128,768]{2,1,0:T(8,128)(2,1)S(1)} async-done(((bf16[16,128,768]{2,1,0:T(8,128)(2,1)}), bf16[16,128,768]{2,1,0:T(8,128)(2,1)S(1)}, u32[]{:S(2)}, u32[]{:S(2)}) %all-to-all-start.2) | async-done | bytes 3145760 | tf_op jit(solution)/shard_map/all_to_all | solution.py:58
  111.5 4.5 %convert_reduce_fusion.2 = (f32[1024]{0:T(1024)S(1)}, f32[1024]{0:T(1024)S(1)}, bf16[1024,256]{1,0:T(8,128)(2,1)}) fusion(f32[256]{0:T(256)S(1)} %copy-done.11, bf16[1024,2048]{1,0:T(8,128)(2,1)} %bitcast.59, bf16[2048,768]{1,0:T(8,128)(2,1)S(1)} %bitcast.65), kind=kOutput, calls=%fused_computation.17 | convolution fusion | flops 1077409792 | bytes 5776384 | tf_op jit(solution)/shard_map/dot_general | solution.py:136
  116.6 4.5 %all-to-all-start.3 = ((f32[8,1,2048]{2,1,0:T(1,128)}), f32[8,1,2048]{2,1,0:T(1,128)S(1)}, u32[]{:S(2)}, u32[]{:S(2)}) async-start(f32[8,1,2048]{2,1,0:T(1,128)} %broadcast_in_dim.15), calls=%async_computation.3 | async-start | bytes 131072 | tf_op jit(solution)/shard_map/all_to_all | solution.py:16
  121.1 4.4 %fusion.24 = bf16[1024,256]{1,0:T(8,128)(2,1)} fusion(bf16[1024,2048]{1,0:T(8,128)(2,1)} %bitcast.60, bf16[2048,768]{1,0:T(8,128)(2,1)S(1)} %bitcast.66, f32[256]{0:T(256)S(1)} %copy-done.12), kind=kOutput, calls=%fused_computation.41 | convolution fusion | flops 1076363264 | bytes 5768192 | tf_op jit(solution)/shard_map/dot_general | solution.py:135
  130.7 8.6 %all_to_all.62 = bf16[2,4,128,2048]{3,2,1,0:T(8,128)(2,1)} all-to-all(bf16[2,4,128,2048]{3,2,1,0:T(8,128)(2,1)S(1)} %bitcast.57), channel_id=1, replica_groups=mesh['fs'=16,'tp_0'=4,'tp_1'=2] {'tp_1'}, dimensions={0} | all-to-all | bytes 8388608 | tf_op jit(solution)/shard_map/all_to_all | solution.py:41
  142.8 28.7 %all_to_all.63 = bf16[4,128,2048]{2,1,0:T(8,128)(2,1)S(1)} all-to-all(bf16[4,128,2048]{2,1,0:T(8,128)(2,1)S(1)} %reduce_sum.91), channel_id=1, replica_groups=mesh['fs'=16,'tp_0'=4,'tp_1'=2] {'tp_0'}, dimensions={0} | all-to-all | bytes 4194304 | tf_op jit(solution)/shard_map/all_to_all | solution.py:49
  174.1 3.6 all-to-all-start.7
  182.2 20.1 %all-to-all-done.7 = bf16[4,128,2048]{2,1,0:T(8,128)(2,1)S(1)} async-done(((bf16[4,128,2048]{2,1,0:T(8,128)(2,1)}), bf16[4,128,2048]{2,1,0:T(8,128)(2,1)S(1)}, u32[]{:S(2)}, u32[]{:S(2)}) %all-to-all-start.7) | async-done | bytes 2097184 | tf_op jit(solution)/shard_map/all_to_all | solution.py:16
  202.8 10.5 %all_to_all.64 = bf16[2,4,128,2048]{3,2,1,0:T(8,128)(2,1)} all-to-all(bf16[2,4,128,2048]{3,2,1,0:T(8,128)(2,1)S(1)} %broadcast_in_dim.18), channel_id=1, replica_groups=mesh['fs'=16,'tp_0'=4,'tp_1'=2] {'tp_1'}, dimensions={0} | all-to-all | bytes 8388608 | tf_op jit(solution)/shard_map/all_to_all | solution.py:16
  213.3 4.6 %stack.8 = bf16[16,128,2304]{2,1,0:T(8,128)(2,1)} broadcast(bf16[128,2304]{1,0:T(8,128)(2,1)S(1)} %copy.61), dimensions={1,2} | broadcast | bytes 10027008 | tf_op jit(solution)/shard_map/stack | solution.py:58
  217.8 5.0 %all-to-all-start.9 = ((bf16[16,128,2304]{2,1,0:T(8,128)(2,1)}), bf16[16,128,2304]{2,1,0:T(8,128)(2,1)}, u32[]{:S(2)}, u32[]{:S(2)}) async-start(bf16[16,128,2304]{2,1,0:T(8,128)(2,1)} %stack.8), calls=%async_computation.9 | async-start | bytes 18874368 | tf_op jit(solution)/shard_map/all_to_all | solution.py:58
  222.8 4.8 %copy.58 = bf16[2,4,128,2048]{3,2,0,1:T(8,128)(2,1)} copy(bf16[2,4,128,2048]{3,2,1,0:T(8,128)(2,1)} %all_to_all.64) | data formatting | bytes 8388608 | tf_op jit(solution)/shard_map/all_to_all | solution.py:16
  227.6 136.6 %all-to-all-done.9 = bf16[16,128,2304]{2,1,0:T(8,128)(2,1)} async-done(((bf16[16,128,2304]{2,1,0:T(8,128)(2,1)}), bf16[16,128,2304]{2,1,0:T(8,128)(2,1)}, u32[]{:S(2)}, u32[]{:S(2)}) %all-to-all-start.9) | async-done | bytes 9437216 | tf_op jit(solution)/shard_map/all_to_all | solution.py:58
  364.1 8.2 %fusion.1 = f32[1024,768]{1,0:T(8,128)} fusion(bf16[1024,2048]{1,0:T(8,128)(2,1)} %bitcast.61, bf16[2048,2304]{1,0:T(8,128)(2,1)} %bitcast.22), kind=kOutput, calls=%fused_computation.7 | convolution fusion | flops 3221225472 | bytes 10485760 | tf_op jit(solution)/shard_map/dot_general | solution.py:185
  372.4 13.3 %multiply_convert_fusion = bf16[1024,2048]{1,0:T(8,128)(2,1)} fusion(f32[2048]{0:T(1024)S(1)} %bitcast.72, bf16[2048,2304]{1,0:T(8,128)(2,1)} %bitcast.22, f32[1024,768]{1,0:T(8,128)} %fusion.1, bf16[1024,2048]{1,0:T(8,128)(2,1)} %bitcast.62, f32[768]{0:T(1024)S(1)} %copy-done.9, f32[768]{0:T(1024)S(1)} %copy-done.10), kind=kOutput, calls=%fused_computation | convolution fusion | flops 6452936704 | bytes 17840128 | tf_op jit(solution)/shard_map/dot_general | solution.py:191
  388.2 9.0 %all_to_all.65 = bf16[2,4,128,2048]{3,2,1,0:T(8,128)(2,1)} all-to-all(bf16[2,4,128,2048]{3,2,1,0:T(8,128)(2,1)S(1)} %bitcast.58), channel_id=1, replica_groups=mesh['fs'=16,'tp_0'=4,'tp_1'=2] {'tp_1'}, dimensions={0} | all-to-all | bytes 8388608 | tf_op jit(solution)/shard_map/all_to_all | solution.py:41
  400.8 28.5 %all_to_all.66 = bf16[4,128,2048]{2,1,0:T(8,128)(2,1)S(1)} all-to-all(bf16[4,128,2048]{2,1,0:T(8,128)(2,1)S(1)} %reduce_sum.94), channel_id=1, replica_groups=mesh['fs'=16,'tp_0'=4,'tp_1'=2] {'tp_0'}, dimensions={0} | all-to-all | bytes 4194304 | tf_op jit(solution)/shard_map/all_to_all | solution.py:49
  (66 shorter events, 32.6 us)
Async XLA Ops:
  0.0 63.4 %copy-start = (f32[8,128]{1,0:T(8,128)S(1)}, f32[8,128]{1,0:T(8,128)}, u32[]{:S(2)}) copy-start(f32[8,128]{1,0:T(8,128)} %param.27) | copy-start | bytes 12292
  1.3 14.9 %all-to-all-start.4 = ((f32[16,128,2]{1,2,0:T(2,128)}), f32[16,128,2]{1,2,0:T(2,128)S(1)}, u32[]{:S(2)}, u32[]{:S(2)}) async-start(f32[16,128,2]{1,2,0:T(2,128)} %stack.7), calls=%async_computation.4 | async-start | bytes 32768 | tf_op jit(solution)/shard_map/all_to_all | solution.py:58
  12.2 9.8 %copy-start.4 = (f32[128,256]{1,0:T(8,128)S(1)}, f32[128,256]{1,0:T(8,128)}, u32[]{:S(2)}) copy-start(f32[128,256]{1,0:T(8,128)} %param.23) | copy-start | bytes 393220
  12.2 9.9 %copy-start.5 = (f32[128,256]{1,0:T(8,128)S(1)}, f32[128,256]{1,0:T(8,128)}, u32[]{:S(2)}) copy-start(f32[128,256]{1,0:T(8,128)} %param.21) | copy-start | bytes 393220
  12.2 10.0 %copy-start.6 = (f32[256,128]{1,0:T(8,128)S(1)}, f32[256,128]{1,0:T(8,128)}, u32[]{:S(2)}) copy-start(f32[256,128]{1,0:T(8,128)} %param.28) | copy-start | bytes 393220
  17.8 28.2 %all-to-all-start = ((bf16[4,128,2048]{2,1,0:T(8,128)(2,1)}), bf16[4,128,2048]{2,1,0:T(8,128)(2,1)S(1)}, u32[]{:S(2)}, u32[]{:S(2)}) async-start(bf16[4,128,2048]{2,1,0:T(8,128)(2,1)} %broadcast_in_dim.13), calls=%async_computation | async-start | bytes 4194304 | tf_op jit(solution)/shard_map/all_to_all | solution.py:16
  59.6 51.9 %all-to-all-start.2 = ((bf16[16,128,768]{2,1,0:T(8,128)(2,1)}), bf16[16,128,768]{2,1,0:T(8,128)(2,1)S(1)}, u32[]{:S(2)}, u32[]{:S(2)}) async-start(bf16[16,128,768]{2,1,0:T(8,128)(2,1)} %stack.6), calls=%async_computation.2 | async-start | bytes 6291456 | tf_op jit(solution)/shard_map/all_to_all | solution.py:58
  63.4 48.1 %copy-start.11 = (f32[256]{0:T(256)S(1)}, f32[256]{0:T(256)}, u32[]{:S(2)}) copy-start(f32[256]{0:T(256)} %param.24) | copy-start | bytes 3076
  111.5 9.6 %copy-start.12 = (f32[256]{0:T(256)S(1)}, f32[256]{0:T(256)}, u32[]{:S(2)}) copy-start(f32[256]{0:T(256)} %param.22) | copy-start | bytes 3076
  116.6 9.4 %all-to-all-start.3 = ((f32[8,1,2048]{2,1,0:T(1,128)}), f32[8,1,2048]{2,1,0:T(1,128)S(1)}, u32[]{:S(2)}, u32[]{:S(2)}) async-start(f32[8,1,2048]{2,1,0:T(1,128)} %broadcast_in_dim.15), calls=%async_computation.3 | async-start | bytes 131072 | tf_op jit(solution)/shard_map/all_to_all | solution.py:16
  121.1 4.9 %copy-start.8 = (f32[256]{0:T(256)S(1)}, f32[256]{0:T(256)}, u32[]{:S(2)}) copy-start(f32[256]{0:T(256)} %param.25) | copy-start | bytes 3076
  142.8 29.1 %copy-start.2 = (bf16[128,2048]{1,0:T(8,128)(2,1)S(1)}, bf16[128,2048]{1,0:T(8,128)(2,1)}, u32[]{:S(2)}) copy-start(bf16[128,2048]{1,0:T(8,128)(2,1)} %param.18) | copy-start | bytes 1572868
  171.6 0.7 copy-start.7
  172.5 5.2 %copy-start.3 = (f32[128,768]{1,0:T(8,128)S(1)}, f32[128,768]{1,0:T(8,128)}, u32[]{:S(2)}) copy-start(f32[128,768]{1,0:T(8,128)} %param.32) | copy-start | bytes 1179652
  174.1 28.2 %all-to-all-start.7 = ((bf16[4,128,2048]{2,1,0:T(8,128)(2,1)}), bf16[4,128,2048]{2,1,0:T(8,128)(2,1)S(1)}, u32[]{:S(2)}, u32[]{:S(2)}) async-start(bf16[4,128,2048]{2,1,0:T(8,128)(2,1)} %broadcast_in_dim.17), calls=%async_computation.7 | async-start | bytes 4194304 | tf_op jit(solution)/shard_map/all_to_all | solution.py:16
  217.8 146.3 %all-to-all-start.9 = ((bf16[16,128,2304]{2,1,0:T(8,128)(2,1)}), bf16[16,128,2304]{2,1,0:T(8,128)(2,1)}, u32[]{:S(2)}, u32[]{:S(2)}) async-start(bf16[16,128,2304]{2,1,0:T(8,128)(2,1)} %stack.8), calls=%async_computation.9 | async-start | bytes 18874368 | tf_op jit(solution)/shard_map/all_to_all | solution.py:58
  364.1 8.2 %copy-start.9 = (f32[768]{0:T(1024)S(1)}, f32[768]{0:T(1024)}, u32[]{:S(2)}) copy-start(f32[768]{0:T(1024)} %param.33) | copy-start | bytes 9220
  364.1 8.2 %copy-start.10 = (f32[768]{0:T(1024)S(1)}, f32[768]{0:T(1024)}, u32[]{:S(2)}) copy-start(f32[768]{0:T(1024)} %param.31) | copy-start | bytes 9220
  400.8 29.9 %copy-start.1 = (f32[8,128]{1,0:T(8,128)S(1)}, f32[8,128]{1,0:T(8,128)}, u32[]{:S(2)}) copy-start(f32[8,128]{1,0:T(8,128)} %param.27) | copy-start | bytes 12292
